TPU v7x, 32 devices: a whole 2x2x4 slice. The times are simulated.
32 devices in a mesh: ep: 8 (over z, core), tp: 4 (over y, x).
Axes of the slice: x: 2, y: 2, z: 4, core: 2. Of those that a mesh axis runs over, the one named last changes fastest.
Arguments:
- receptance: bfloat16 [2048, 2048], P('ep', 'tp'), may hold values from -6 to 6
- key_tensor: bfloat16 [2048, 2048], P('ep', 'tp'), may hold values from -6 to 6
- value_tensor: bfloat16 [2048, 2048], P('ep', 'tp'), may hold values from -6 to 6
- decay_data_input: bfloat16 [2048, 2048], P('ep', 'tp'), may hold values from -4 to 4
- correction_rate_input: bfloat16 [2048, 2048], P('ep', 'tp'), may hold values from -16 to 6
- mixer_output_gate: bfloat16 [2048, 2048], P('ep', 'tp'), may hold values from -6 to 6
- decay_channel_offset: float32 [2048], P('tp'), may hold values from -16 to -3
- head_norm_gain: float32 [2048], P('tp'), may hold values from 0.1 to 1.9
- self_key_weight: float32 [2048], P('tp'), may hold values from -2 to 2
- mixer_output_weight: bfloat16 [2048, 2048], P('tp'), may hold values from -0.125 to 0.125
- second_batch_rows: bfloat16 [1024, 2048], P('ep'), may hold values from -6 to 6
- routed_expert_index: int32 [1024, 4], P('ep'), may hold values from 0 to 7, all different within a row; in each aligned block of 128 rows (0 to 127, 128 to 255, ...) at most 96 rows name the same one
- routing_output_weight: float32 [1024, 4], P('ep'), may hold values from 0.1 to 1
- expert_norm_gain: float32 [2048], replicated, may hold values from 0.1 to 1.9
- expert_gate_weight: bfloat16 [8, 1024, 2048], P('ep', 'tp'), may hold values from -0.125 to 0.125
- expert_up_weight: bfloat16 [8, 1024, 2048], P('ep', 'tp'), may hold values from -0.125 to 0.125
- expert_down_weight: bfloat16 [8, 1024, 2048], P('ep', None, 'tp'), may hold values from -0.1875 to 0.1875
- common_expert_gate: bfloat16 [1024, 2048], P('tp'), may hold values from -0.125 to 0.125
- common_expert_up: bfloat16 [1024, 2048], P('tp'), may hold values from -0.125 to 0.125
- common_expert_down: bfloat16 [1024, 2048], P(None, 'tp'), may hold values from -0.1875 to 0.1875
Outputs:
- token_mixer_output: bfloat16 [2048, 2048], P(('ep', 'tp'))
- expert_out: bfloat16 [1024, 2048], P('ep', 'tp')
Inputs may be any that keep to these rules, and one draw needn't show every extreme that they name: `routed_expert_index`: each row names 4 different experts. Within the rows of one index of ep no expert is named by more than 96 rows, and that bound is met in some index's rows.
All inputs are finite; a program needn't handle non-finite values.
Results may differ from a plain program's by a relative error of at most 0.017.
Values may be sent and summed in bfloat16 or wider, within the bound.
A program may use at most 128 MiB of HBM per device.

v0:
```python
import math
import jax
import jax.numpy as jnp
from jax import lax
from jax.sharding import PartitionSpec as P

HEAD_CHANNELS = 64
SPAN = 64
HIGHEST = lax.Precision.HIGHEST
PRECISION = lax.Precision.HIGH
NORM_FLOOR = 1.0


def head_view(matrix):
    return matrix.astype(jnp.float32).reshape(matrix.shape[0], -1, HEAD_CHANNELS)


def complete_head_outputs(
    state_readout,
    receptance_rows,
    key_row_block,
    value_row_block,
    head_norm_gain,
    self_key_weight,
    mixer_output_gate,
):
    mean_part = jnp.mean(state_readout, axis=-1, keepdims=True)
    spread = jnp.mean(jnp.square(state_readout - mean_part), axis=-1, keepdims=True)
    normalized_rows = (state_readout - mean_part) * lax.rsqrt(spread + NORM_FLOOR)
    sequence_length = state_readout.shape[0]
    normalized_rows = normalized_rows.reshape(sequence_length, -1) * head_norm_gain
    self_key_term = (
        jnp.sum(
            receptance_rows * key_row_block * self_key_weight.reshape(-1, HEAD_CHANNELS),
            axis=-1,
            keepdims=True,
        )
        * value_row_block
    )
    mixer_result = (
        normalized_rows + self_key_term.reshape(sequence_length, -1)
    ) * mixer_output_gate.astype(jnp.float32)
    return mixer_result.astype(jnp.bfloat16)


def product(spec, left, right):
    return jnp.einsum(spec, left, right, precision=PRECISION, preferred_element_type=jnp.float32)


def lower_inverse(strict, size):
    at = jnp.arange(size)
    row, column = (at[:, None], at[None, :])
    inverse = None
    block = 1
    while block < size:
        pair = (
            (row // (2 * block) == column // (2 * block))
            & (row // block % 2 == 1)
            & (column // block % 2 == 0)
        )
        below = jnp.where(pair, strict, 0.0)
        if inverse is None:
            inverse = jnp.eye(size, dtype=jnp.float32) - below
        else:
            inverse = inverse - product(
                "nhij,nhjk->nhik", product("nhij,nhjk->nhik", inverse, below), inverse
            )
        block *= 2
    return inverse


def mixer_part(
    receptance,
    key_tensor,
    value_tensor,
    decay_data_input,
    correction_rate_input,
    mixer_output_gate,
    decay_channel_offset,
    head_norm_gain,
    self_key_weight,
    mixer_output_weight,
    routed_pieces,
):
    row_count, width = receptance.shape
    head_count = width // HEAD_CHANNELS
    span = min(SPAN, row_count)
    block_count = row_count // span
    receptance_rows = head_view(receptance)
    key_row_block = head_view(key_tensor)
    value_row_block = head_view(value_tensor)

    def by_block(matrix):
        return (
            matrix.astype(jnp.float32)
            .reshape(block_count, span, head_count, HEAD_CHANNELS)
            .transpose(0, 2, 1, 3)
        )

    step_log = -math.exp(-0.5) * jax.nn.sigmoid(
        decay_channel_offset + decay_data_input.astype(jnp.float32)
    )
    at = jnp.arange(span)
    reach = (at[:, None] >= at[None, :]).astype(jnp.float32)
    step_log = by_block(step_log)
    total_log = jnp.einsum("ts,nhsd->nhtd", reach, step_log, precision=HIGHEST)
    recept, keys, values = (by_block(receptance), by_block(key_tensor), by_block(value_tensor))
    units = keys * lax.rsqrt(jnp.sum(keys * keys, axis=-1, keepdims=True) + 1.0)
    corrections = units * jax.nn.sigmoid(by_block(correction_rate_input))
    grown = jnp.exp(-total_log)
    last_log = total_log[:, :, -1:, :]
    unit_in = units * jnp.exp(total_log - step_log)
    recept_in = recept * jnp.exp(total_log)
    tail = jnp.exp(last_log - total_log)
    scores = product(
        "nhtd,nhsd->nhts",
        jnp.concatenate([unit_in, recept_in], axis=2),
        jnp.concatenate([keys * grown, corrections * grown], axis=2),
    )
    before = at[:, None] > at[None, :]
    upto = at[:, None] >= at[None, :]
    unit_key = jnp.where(before, scores[:, :, :span, :span], 0.0)
    unit_fix = jnp.where(before, scores[:, :, :span, span:], 0.0)
    read_key = jnp.where(upto, scores[:, :, span:, :span], 0.0)
    read_fix = jnp.where(upto, scores[:, :, span:, span:], 0.0)
    inverse = lower_inverse(unit_fix, span)
    key_values = product("nhts,nhsd->nhtd", jnp.concatenate([unit_key, read_key], axis=2), values)
    solved = product(
        "nhts,nhsd->nhtd", inverse, jnp.concatenate([unit_in, key_values[:, :, :span]], axis=3)
    )
    reads = jnp.concatenate([recept_in, key_values[:, :, span:]], axis=3) - product(
        "nhts,nhsd->nhtd", read_fix, solved
    )
    eye_head = jnp.eye(HEAD_CHANNELS, dtype=jnp.float32)
    fresh = product("nhtj,nhti->nhji", keys * tail, values)
    moves = jnp.concatenate([eye_head * jnp.exp(last_log), fresh], axis=3) - product(
        "nhtj,nhti->nhji", corrections * tail, solved
    )
    whole = moves[0]
    for block in range(1, block_count):
        step = product("hij,hjk->hik", moves[block, :, :, :HEAD_CHANNELS], whole)
        whole = step + jnp.concatenate(
            [jnp.zeros_like(step[..., :HEAD_CHANNELS]), moves[block, :, :, HEAD_CHANNELS:]], axis=2
        )
    whole, routed_pieces = lax.optimization_barrier((whole, routed_pieces))
    everything = lax.all_gather(whole.astype(jnp.bfloat16), "ep")
    mine = lax.axis_index("ep")
    state = jnp.zeros((head_count, HEAD_CHANNELS, HEAD_CHANNELS), jnp.float32)
    for k in range(lax.axis_size("ep") - 1):
        part = everything[k].astype(jnp.float32)
        new = product("hij,hjk->hik", part[..., :HEAD_CHANNELS], state)
        state = jnp.where(k < mine, new + part[..., HEAD_CHANNELS:], state)
    starts = [state]
    for block in range(block_count - 1):
        state = (
            product("hij,hjk->hik", moves[block, :, :, :HEAD_CHANNELS], state)
            + moves[block, :, :, HEAD_CHANNELS:]
        )
        starts.append(state)
    merged_output = reads[..., HEAD_CHANNELS:] + product(
        "nhtj,nhji->nhti", reads[..., :HEAD_CHANNELS], jnp.stack(starts)
    )
    merged_output = merged_output.transpose(0, 2, 1, 3).reshape(
        row_count, head_count, HEAD_CHANNELS
    )
    mixer_result = complete_head_outputs(
        merged_output,
        receptance_rows,
        key_row_block,
        value_row_block,
        head_norm_gain,
        self_key_weight,
        mixer_output_gate,
    )
    summed = lax.psum_scatter(
        jnp.dot(mixer_result, mixer_output_weight, preferred_element_type=jnp.float32).astype(
            jnp.bfloat16
        ),
        "tp",
        scatter_dimension=0,
        tiled=True,
    )
    return (summed, routed_pieces)


def activate(rows_in, gate_part, up_part):
    pre_gate = jnp.einsum("fd,rd->fr", gate_part, rows_in, preferred_element_type=jnp.float32)
    pre_up = jnp.einsum("fd,rd->fr", up_part, rows_in, preferred_element_type=jnp.float32)
    return (jax.nn.silu(pre_gate) * pre_up).astype(jnp.bfloat16)


def expert_entry(
    second_batch_rows,
    routed_expert_index,
    routing_output_weight,
    expert_norm_gain,
    common_expert_gate,
    common_expert_up,
):
    row_count, width = second_batch_rows.shape
    top_count = routed_expert_index.shape[1]
    peer_count = lax.axis_size("ep")
    slot_count = 3 * row_count * top_count // (2 * peer_count)
    widened = second_batch_rows.astype(jnp.float32)
    normalized_rows = (
        widened
        * lax.rsqrt(jnp.mean(widened * widened, axis=-1, keepdims=True) + NORM_FLOOR)
        * expert_norm_gain
    ).astype(jnp.bfloat16)
    flat_ids = routed_expert_index.reshape(-1)
    one_hot = (flat_ids[:, None] == jnp.arange(peer_count, dtype=jnp.int32)[None, :]).astype(
        jnp.int32
    )
    slot_rank = jnp.sum((jnp.cumsum(one_hot, axis=0) - 1) * one_hot, axis=1)
    target = flat_ids * slot_count + slot_rank
    owners = jnp.arange(row_count * top_count, dtype=jnp.int32) // top_count
    source_row = jnp.full((peer_count * slot_count,), row_count, jnp.int32).at[target].set(owners)
    padded = jnp.concatenate([normalized_rows, jnp.zeros((1, width), jnp.bfloat16)], axis=0)
    outgoing = jnp.take(padded, source_row, axis=0).reshape(peer_count, slot_count, width)
    shared_hidden = activate(normalized_rows, common_expert_gate, common_expert_up)
    piece_width = width // lax.axis_size("tp")
    own_slice = lax.dynamic_slice_in_dim(
        outgoing, lax.axis_index("tp") * piece_width, piece_width, 2
    )
    arrived = lax.all_to_all(own_slice, "ep", split_axis=0, concat_axis=0, tiled=True)
    return (arrived, shared_hidden, target)


def expert_exit(
    slots,
    pieces,
    shared_hidden,
    target,
    routing_output_weight,
    expert_gate_weight,
    expert_up_weight,
    expert_down_weight,
    common_expert_down,
):
    peer_count, slot_count = slots
    row_count, top_count = routing_output_weight.shape
    out_width = expert_down_weight.shape[2]
    gate_cols = expert_gate_weight[0]
    up_cols = expert_up_weight[0]
    pre_gate = jnp.einsum("fd,rd->fr", gate_cols, pieces, preferred_element_type=jnp.float32)
    pre_up = jnp.einsum("fd,rd->fr", up_cols, pieces, preferred_element_type=jnp.float32)
    routed_hidden = (jax.nn.silu(pre_gate) * pre_up).astype(jnp.bfloat16)
    both = lax.all_gather(
        jnp.concatenate([routed_hidden, shared_hidden], axis=1), "tp", axis=0, tiled=True
    )
    pieces = (both[:, : routed_hidden.shape[1]], both[:, routed_hidden.shape[1] :])
    routed_rows = expert_down_weight[0]
    routed_sum = jnp.einsum("fr,fd->rd", pieces[0], routed_rows, preferred_element_type=jnp.float32)
    shared_out = jnp.einsum(
        "fr,fd->rd", pieces[1], common_expert_down, preferred_element_type=jnp.float32
    )
    returned = lax.all_to_all(
        routed_sum.astype(jnp.bfloat16).reshape(peer_count, slot_count, out_width),
        "ep",
        split_axis=0,
        concat_axis=0,
        tiled=True,
    )
    picked = jnp.take(returned.reshape(-1, out_width), target, axis=0).reshape(
        row_count, top_count, out_width
    )
    merged_output = (
        jnp.sum(picked.astype(jnp.float32) * routing_output_weight[:, :, None], axis=1) + shared_out
    )
    return merged_output.astype(jnp.bfloat16)


def on_device(
    receptance,
    key_tensor,
    value_tensor,
    decay_data_input,
    correction_rate_input,
    mixer_output_gate,
    decay_channel_offset,
    head_norm_gain,
    self_key_weight,
    mixer_output_weight,
    second_batch_rows,
    routed_expert_index,
    routing_output_weight,
    expert_norm_gain,
    expert_gate_weight,
    expert_up_weight,
    expert_down_weight,
    common_expert_gate,
    common_expert_up,
    common_expert_down,
):
    arrived, shared_hidden, target = expert_entry(
        second_batch_rows,
        routed_expert_index,
        routing_output_weight,
        expert_norm_gain,
        common_expert_gate,
        common_expert_up,
    )
    arrived, receptance, key_tensor, value_tensor, decay_data_input, correction_rate_input = (
        lax.optimization_barrier(
            (arrived, receptance, key_tensor, value_tensor, decay_data_input, correction_rate_input)
        )
    )
    flat_rows = arrived.reshape(-1, arrived.shape[2])
    pieces = lax.all_gather(flat_rows, "tp", axis=1, tiled=True)
    token_mixer_output, pieces = mixer_part(
        receptance,
        key_tensor,
        value_tensor,
        decay_data_input,
        correction_rate_input,
        mixer_output_gate,
        decay_channel_offset,
        head_norm_gain,
        self_key_weight,
        mixer_output_weight,
        pieces,
    )
    expert_out = expert_exit(
        arrived.shape[:2],
        pieces,
        shared_hidden,
        target,
        routing_output_weight,
        expert_gate_weight,
        expert_up_weight,
        expert_down_weight,
        common_expert_down,
    )
    return (token_mixer_output, expert_out)


def solution(mesh):
    in_specs = (
        P("ep", "tp"),
        P("ep", "tp"),
        P("ep", "tp"),
        P("ep", "tp"),
        P("ep", "tp"),
        P("ep", "tp"),
        P("tp"),
        P("tp"),
        P("tp"),
        P("tp", None),
        P("ep", None),
        P("ep", None),
        P("ep", None),
        P(),
        P("ep", "tp", None),
        P("ep", "tp", None),
        P("ep", None, "tp"),
        P("tp", None),
        P("tp", None),
        P(None, "tp"),
    )
    out_specs = (P(("ep", "tp"), None), P("ep", "tp"))
    return jax.shard_map(
        on_device, mesh=mesh, in_specs=in_specs, out_specs=out_specs, check_vma=False
    )
```

profile of v0, /device:TPU:0, one launch (start us, length us, event | category | flops | bytes accessed | tf_op | source)
XLA Modules:
  0.0 222.1 jit_solution(11237634688748817533)
XLA Ops:
  10.8 2.4 %scatter_custom_fusion = s32[768]{0:T(1024)S(1)} fusion(s32[512]{0:T(512)S(1)} %bitcast.191, s32[512]{0:T(512)S(1)} %add_select_fusion, s32[]{:T(128)} %constant.328.clone.1), kind=kCustom, calls=%fused_computation.207 | custom fusion | bytes 3076 | tf_op jit(solution)/shard_map/scatter | solution.py:217
  15.9 4.3 %gather_fusion = bf16[768,2048]{1,0:T(8,128)(2,1)} fusion(bf16[129,2048]{1,0:T(8,128)(2,1)S(1)} %concatenate.33, s32[1024]{0:T(1024)S(1)} %pad_clamp_fusion.1), kind=kCustom, calls=%fused_computation | custom fusion | bytes 6294528 | tf_op jit(solution)/shard_map/jit(_take)/gather | solution.py:219
  20.2 2.3 %dynamic-slice_select_fusion = bf16[8,96,512]{2,1,0:T(8,128)(2,1)} fusion(bf16[8,96,2048]{2,1,0:T(8,128)(2,1)} %bitcast.177, s32[]{:T(128)S(6)} %select_n.364, pred[8,96]{1,0:T(8,128)(4,1)S(1)} %broadcast_in_dim.94), kind=kLoop, calls=%fused_computation.114 | loop fusion | flops 393216 | bytes 1573636 | tf_op jit(solution)/shard_map/jit(_take)/select_n | solution.py:219
  22.4 6.5 %all-to-all-start = ((bf16[8,96,512]{2,1,0:T(8,128)(2,1)}), bf16[8,96,512]{2,1,0:T(8,128)(2,1)}, u32[]{:S(2)}, u32[]{:S(2)}) async-start(bf16[8,96,512]{2,1,0:T(8,128)(2,1)} %dynamic-slice_select_fusion), calls=%async_computation | async-start | bytes 1572864 | tf_op jit(solution)/shard_map/all_to_all | solution.py:225
  29.9 2.4 %convolution_bitcast_fusion.4 = f32[256,128]{0,1:T(8,128)} fusion(bf16[128,2048]{1,0:T(8,128)(2,1)S(1)} %fusion.33, bf16[256,2048]{1,0:T(8,128)(2,1)} %param.37), kind=kOutput, calls=%fused_computation.60 | convolution fusion | flops 134217728 | bytes 1703936 | tf_op jit(solution)/shard_map/fd,rd->fr/dot_general | solution.py:187
  32.3 17.7 %all-to-all-done = bf16[8,96,512]{2,1,0:T(8,128)(2,1)} async-done(((bf16[8,96,512]{2,1,0:T(8,128)(2,1)}), bf16[8,96,512]{2,1,0:T(8,128)(2,1)}, u32[]{:S(2)}, u32[]{:S(2)}) %all-to-all-start) | async-done | bytes 786464 | tf_op jit(solution)/shard_map/all_to_all | solution.py:225
  51.0 2.1 add_divide_fusion
  57.7 2.3 %reshape.834 = f32[4,64,8,64]{3,2,1,0:T(8,128)} reshape(f32[256,512]{1,0:T(8,128)} %get-tuple-element.35) | data formatting | bytes 1048576 | tf_op jit(solution)/shard_map/reshape | solution.py:96
  59.9 2.4 %reshape.884 = f32[4,64,8,64]{1,0,3,2:T(4,128)} reshape(bf16[256,512]{0,1:T(8,128)(2,1)} %copy.246) | data formatting | bytes 786432 | tf_op jit(solution)/shard_map/reshape | solution.py:96
  62.3 2.6 %copy.248 = f32[4,64,8,64]{3,1,2,0:T(8,128)} copy(f32[4,64,8,64]{1,0,3,2:T(4,128)} %reshape.884) | data formatting | bytes 1048576 | tf_op jit(solution)/shard_map/reshape | solution.py:96
  64.8 5.0 %fusion.66 = (f32[4,8,64,64]{3,2,1,0:T(8,128)S(1)}, f32[4,8,64,64]{3,2,1,0:T(8,128)S(1)}, f32[4,8,64,64]{3,2,1,0:T(8,128)S(1)}, f32[4,8,64,64]{3,2,1,0:T(8,128)S(1)}, f32[4,8,64,64]{3,2,1,0:T(8,128)}) fusion(f32[4,64,8,64]{3,2,1,0:T(8,128)} %reshape.842, f32[4,8,64]{2,1,0:T(8,128)S(1)} %add_rsqrt_fusion.1, f32[4,64,8,64]{3,1,2,0:T(8,128)S(1)} %copy.252, ...), kind=kOutput, calls=%fused_computation.113 | convolution fusion | flops 101715968 | bytes 4726784 | tf_op jit(solution)/shard_map/ts,nhsd->nhtd/dot_general | solution.py:106
  69.8 2.3 %fusion.1 = f32[4,8,128,128]{3,2,1,0:T(8,128)S(1)} fusion(f32[4,8,64,64]{3,2,1,0:T(8,128)S(1)} %get-tuple-element.30, f32[4,8,64,64]{3,2,1,0:T(8,128)S(1)} %get-tuple-element.19, f32[4,8,64,64]{3,2,1,0:T(8,128)S(1)} %get-tuple-element.18, f32[4,8,64,64]{3,2,1,0:T(8,128)S(1)} %get-tuple-element.24), kind=kOutput, calls=%fused_computation.5 | convolution fusion | flops 201850880 | bytes 4194304 | tf_op jit(solution)/shard_map/nhtd,nhsd->nhts/dot_general | solution.py:47
  79.9 2.6 %fusion.8 = f32[4,8,128,64]{3,2,1,0:T(8,128)S(1)} fusion(f32[4,8,64,64]{3,2,1,0:T(8,128)} %get-tuple-element.23, f32[4,8,64,64]{3,2,1,0:T(8,128)} %get-tuple-element.22, bf16[4,8,64,64]{3,1,2,0:T(8,128)(2,1)} %bitcast.178), kind=kOutput, calls=%fused_computation.12 | convolution fusion | flops 100925440 | bytes 2359296 | tf_op jit(solution)/shard_map/nhts,nhsd->nhtd/dot_general | solution.py:47
  96.7 25.7 %all-gather.5.cloned.1.call-done = bf16[768,2048]{1,0:T(8,128)(2,1)} async-done(((bf16[768,512]{1,0:T(8,128)(2,1)}), bf16[768,2048]{1,0:T(8,128)(2,1)}) %all-gather.5.cloned.1.call-update) | async-done | bytes 3145744 | tf_op jit(solution)/shard_map/all_gather | solution.py:309
  122.8 2.5 %fusion.30 = bf16[256,128]{0,1:T(8,128)(2,1)} fusion(bf16[128,2048]{1,0:T(8,128)(2,1)} %copy-done.14, bf16[256,2048]{1,0:T(8,128)(2,1)} %param.38, f32[256,128]{0,1:T(8,128)S(1)} %copy-done.19), kind=kOutput, calls=%fused_computation.61 | convolution fusion | flops 134414336 | bytes 1769472 | tf_op jit(solution)/shard_map/fd,rd->fr/dot_general | solution.py:188
  130.1 3.9 %convolution_subtract_fusion.6 = f32[4,8,64,128]{3,2,1,0:T(8,128)} fusion(f32[4,8,64,128]{3,2,1,0:T(8,128)} %copy-done.10, f32[4,8,128,128]{3,2,1,0:T(8,128)} %copy-done.1, f32[4,8,64,64]{3,2,1,0:T(8,128)} %get-tuple-element.20, f32[4,8,64,64]{3,2,1,0:T(8,128)S(1)} %copy-done.9, pred[64,64]{1,0:T(8,128)(4,1)S(1)} %iota_compare_fusion.2), kind=kOutput, calls=%fused_computation.27 | convolution fusion | flops 101318656 | bytes 4722688 | tf_op jit(solution)/shard_map/nhts,nhsd->nhtd/dot_general | solution.py:47
  137.1 9.7 %all-gather.9.cloned.1.call-done = bf16[64,64,128]{2,1,0:T(8,128)(2,1)} async-done(((bf16[8,64,128]{2,1,0:T(8,128)(2,1)}), bf16[64,64,128]{2,1,0:T(8,128)(2,1)}) %all-gather.9.cloned.1.call-update) | async-done | bytes 1048592 | tf_op jit(solution)/shard_map/all_gather | solution.py:146
  159.4 2.1 copy.273
  162.9 3.2 %convolution_convert_fusion = bf16[256,2048]{1,0:T(8,128)(2,1)} fusion(bf16[512,2048]{1,0:T(8,128)(2,1)S(1)} %copy-done, bf16[256,512]{1,0:T(8,128)(2,1)} %param.25, f32[256,512]{1,0:T(8,128)} %copy.274, bf16[256,512]{1,0:T(8,128)(2,1)S(1)} %copy-done.16, f32[256,512]{1,0:T(8,128)} %copy.273, f32[256,512]{1,0:T(8,128)} %reshape.838, ...), kind=kOutput, calls=%fused_computation.4 | convolution fusion | flops 538574848 | bytes 5769216 | tf_op jit(solution)/shard_map/dot_general | solution.py:176
  166.2 15.0 %all-gather.7.cloned.1.call-done = bf16[1024,896]{0,1:T(8,128)(2,1)} async-done(((bf16[256,896]{0,1:T(8,128)(2,1)}), bf16[1024,896]{0,1:T(8,128)(2,1)}) %all-gather.7.cloned.1.call-update) | async-done | bytes 1835024 | tf_op jit(solution)/shard_map/all_gather | solution.py:248
  181.2 3.6 %fusion.14 = bf16[768,512]{1,0:T(8,128)(2,1)} fusion(bf16[1024,896]{0,1:T(8,128)(2,1)} %all-gather.7.cloned.1.call-done, bf16[1,1024,512]{2,1,0:T(8,128)(2,1)} %param.36), kind=kOutput, calls=%fused_computation.23 | convolution fusion | flops 805699584 | bytes 3407872 | tf_op jit(solution)/shard_map/fr,fd->rd/dot_general | solution.py:253
  184.8 4.6 %all-to-all-start.1 = ((bf16[8,96,512]{2,1,0:T(8,128)(2,1)}), bf16[8,96,512]{2,1,0:T(8,128)(2,1)S(1)}, u32[]{:S(2)}, u32[]{:S(2)}) async-start(bf16[8,96,512]{2,1,0:T(8,128)(2,1)} %bitcast.186), calls=%async_computation.2 | async-start | bytes 1572864 | tf_op jit(solution)/shard_map/all_to_all | solution.py:257
  189.8 20.5 %all-to-all-done.1 = bf16[8,96,512]{2,1,0:T(8,128)(2,1)S(1)} async-done(((bf16[8,96,512]{2,1,0:T(8,128)(2,1)}), bf16[8,96,512]{2,1,0:T(8,128)(2,1)S(1)}, u32[]{:S(2)}, u32[]{:S(2)}) %all-to-all-start.1) | async-done | bytes 786464 | tf_op jit(solution)/shard_map/all_to_all | solution.py:257
  213.3 2.3 %fusion.28 = bf16[128,512]{1,0:T(8,128)(2,1)} fusion(f32[128,512]{1,0:T(8,128)S(1)} %multiply_reduce_fusion, bf16[1024,512]{1,0:T(8,128)(2,1)} %param.39, bf16[1024,896]{0,1:T(8,128)(2,1)} %all-gather.7.cloned.1.call-done), kind=kOutput, calls=%fused_computation.57 | convolution fusion | flops 134348800 | bytes 1703936 | tf_op jit(solution)/shard_map/fr,fd->rd/dot_general | solution.py:254
  (175 shorter events, 59.6 us)
Async XLA Ops:
  7.2 155.7 %copy-start = (bf16[512,2048]{1,0:T(8,128)(2,1)S(1)}, bf16[512,2048]{1,0:T(8,128)(2,1)}, u32[]{:S(2)}) copy-start(bf16[512,2048]{1,0:T(8,128)(2,1)} %param.29) | copy-start | bytes 6291460
  15.8 14.1 %copy-start.14 = (bf16[128,2048]{1,0:T(8,128)(2,1)}, bf16[128,2048]{1,0:T(8,128)(2,1)S(1)}, u32[]{:S(2)}) copy-start(bf16[128,2048]{1,0:T(8,128)(2,1)S(1)} %fusion.33) | copy-start | bytes 1572868
  22.4 27.5 %copy-start.17 = (bf16[256,512]{1,0:T(8,128)(2,1)S(1)}, bf16[256,512]{1,0:T(8,128)(2,1)}, u32[]{:S(2)}) copy-start(bf16[256,512]{1,0:T(8,128)(2,1)} %param.21) | copy-start | bytes 786436
  22.4 27.7 %copy-start.18 = (bf16[256,512]{1,0:T(8,128)(2,1)S(1)}, bf16[256,512]{1,0:T(8,128)(2,1)}, u32[]{:S(2)}) copy-start(bf16[256,512]{1,0:T(8,128)(2,1)} %param.20) | copy-start | bytes 786436
  22.4 28.5 %copy-start.22 = (f32[512]{0:T(512)S(1)}, f32[512]{0:T(512)}, u32[]{:S(2)}) copy-start(f32[512]{0:T(512)} %param.26) | copy-start | bytes 6148
  22.4 27.5 %all-to-all-start = ((bf16[8,96,512]{2,1,0:T(8,128)(2,1)}), bf16[8,96,512]{2,1,0:T(8,128)(2,1)}, u32[]{:S(2)}, u32[]{:S(2)}) async-start(bf16[8,96,512]{2,1,0:T(8,128)(2,1)} %dynamic-slice_select_fusion), calls=%async_computation | async-start | bytes 1572864 | tf_op jit(solution)/shard_map/all_to_all | solution.py:225
  28.9 93.5 %all-gather.5.cloned.1.call-start = ((), (), s32[]{:S(2)}) async-start(), calls=%async_computation.3 | async-start | bytes 3932160 | tf_op jit(solution)/shard_map/all_gather | solution.py:309
  72.1 2.9 %copy-start.1 = (f32[4,8,128,128]{3,2,1,0:T(8,128)}, f32[4,8,128,128]{3,2,1,0:T(8,128)S(1)}, u32[]{:S(2)}) copy-start(f32[4,8,128,128]{3,2,1,0:T(8,128)S(1)} %fusion.1) | copy-start | bytes 6291460
  79.6 67.2 %all-gather.9.cloned.1.call-start = ((), (), s32[]{:S(2)}) async-start(), calls=%async_computation.6 | async-start | bytes 1179648 | tf_op jit(solution)/shard_map/all_gather | solution.py:146
  79.9 2.8 %copy-start.2 = (f32[4,8,128,128]{3,2,1,0:T(8,128)S(1)}, f32[4,8,128,128]{3,2,1,0:T(8,128)}, u32[]{:S(2)}) copy-start(f32[4,8,128,128]{3,2,1,0:T(8,128)} %copy-done.1) | copy-start | bytes 6291460
  91.3 3.5 %copy-start.10 = (f32[4,8,64,128]{3,2,1,0:T(8,128)}, f32[4,8,64,128]{3,2,1,0:T(8,128)S(1)}, u32[]{:S(2)}) copy-start(f32[4,8,64,128]{3,2,1,0:T(8,128)S(1)} %fusion.35) | copy-start | bytes 3145732
  94.8 28.0 %copy-start.19 = (f32[256,128]{0,1:T(8,128)S(1)}, f32[256,128]{0,1:T(8,128)}, u32[]{:S(2)}) copy-start(f32[256,128]{0,1:T(8,128)} %convolution_bitcast_fusion.4) | copy-start | bytes 393220
  122.5 7.6 %copy-start.9 = (f32[4,8,64,64]{3,2,1,0:T(8,128)S(1)}, f32[4,8,64,64]{3,2,1,0:T(8,128)}, u32[]{:S(2)}) copy-start(f32[4,8,64,64]{3,2,1,0:T(8,128)} %copy-done.8) | copy-start | bytes 1572868
  122.5 58.7 %all-gather.7.cloned.1.call-start = ((), (), s32[]{:S(2)}) async-start(), calls=%async_computation.5 | async-start | bytes 2293760 | tf_op jit(solution)/shard_map/all_gather | solution.py:248
  130.0 3.9 %copy-start.25 = (bf16[768,2048]{1,0:T(8,128)(2,1)S(1)}, bf16[768,2048]{1,0:T(8,128)(2,1)}, u32[]{:S(2)}) copy-start(bf16[768,2048]{1,0:T(8,128)(2,1)} %all-gather.5.cloned.1.call-done) | copy-start | bytes 9437188
  130.0 3.9 %copy-start.26 = (bf16[1,256,2048]{2,1,0:T(8,128)(2,1)S(1)}, bf16[1,256,2048]{2,1,0:T(8,128)(2,1)}, u32[]{:S(2)}) copy-start(bf16[1,256,2048]{2,1,0:T(8,128)(2,1)} %param.34) | copy-start | bytes 3145732
  137.1 18.3 %copy-start.4 = (f32[4,8,64,128]{3,2,1,0:T(8,128)S(1)}, f32[4,8,64,128]{3,2,1,0:T(8,128)}, u32[]{:S(2)}) copy-start(f32[4,8,64,128]{3,2,1,0:T(8,128)} %copy-done.3) | copy-start | bytes 3145732
  137.1 78.5 %reduce-scatter.2.cloned.1.call-start = ((), (), s32[]{:S(2)}) async-start(), calls=%async_computation.4 | async-start | bytes 1310720 | tf_op jit(solution)/shard_map/reduce_scatter | solution.py:175
  151.7 4.5 %copy-start.15 = (f32[4,8,64,128]{3,2,1,0:T(8,128)S(1)}, f32[4,8,64,128]{3,2,1,0:T(8,128)}, u32[]{:S(2)}) copy-start(f32[4,8,64,128]{3,2,1,0:T(8,128)} %convolution_subtract_fusion.6) | copy-start | bytes 3145732
  159.4 3.5 %copy-start.16 = (bf16[256,512]{1,0:T(8,128)(2,1)S(1)}, bf16[256,512]{1,0:T(8,128)(2,1)}, u32[]{:S(2)}) copy-start(bf16[256,512]{1,0:T(8,128)(2,1)} %param.22) | copy-start | bytes 786436
  159.4 3.5 %copy-start.23 = (f32[512]{0:T(512)S(1)}, f32[512]{0:T(512)}, u32[]{:S(2)}) copy-start(f32[512]{0:T(512)} %param.27) | copy-start | bytes 6148
  166.2 23.3 %copy-start.24 = (f32[128,4]{0,1:T(4,128)S(1)}, f32[128,4]{0,1:T(4,128)}, u32[]{:S(2)}) copy-start(f32[128,4]{0,1:T(4,128)} %param.32) | copy-start | bytes 6148
  166.2 23.5 %copy-start.21 = (s32[128,4]{0,1:T(4,128)S(1)}, s32[128,4]{0,1:T(4,128)}, u32[]{:S(2)}) copy-start(s32[128,4]{0,1:T(4,128)} %param.31) | copy-start | bytes 6148
  184.8 25.5 %all-to-all-start.1 = ((bf16[8,96,512]{2,1,0:T(8,128)(2,1)}), bf16[8,96,512]{2,1,0:T(8,128)(2,1)S(1)}, u32[]{:S(2)}, u32[]{:S(2)}) async-start(bf16[8,96,512]{2,1,0:T(8,128)(2,1)} %bitcast.186), calls=%async_computation.2 | async-start | bytes 1572864 | tf_op jit(solution)/shard_map/all_to_all | solution.py:257
  (10 other events, 16.6 us)
Sparse Core Ops, SparseCore 0:
  79.7 42.6 all-gather.4
  124.6 22.2 all-gather.8
  148.7 32.4 all-gather.6
  184.5 27.9 reduce-scatter.1
where the time goes:
time: 223 us; the launch traced here: 222 us
  waiting for transfers between devices  88.7 us (40%)
  matrix products  53.8 us (24%)
  local copies, waits for them, and re-layouts  37.2 us (17%)
  other arithmetic  15.9 us (7%)
  between operations  14.6 us (7%)
  starting transfers between devices  11.9 us (5%)
    dot_general x30, matrix products, product(): jnp.einsum(spec, left, right, precision=PRECISION, preferred_element_type...  32.8 us
    all_gather x1, waiting for transfers between devices, on_device(): pieces = lax.all_gather(flat_rows, 'tp', axis=1, tiled=True)  25.7 us
    all_to_all x1, waiting for transfers between devices, expert_exit(): lax.all_to_all(routed_sum.astype(jnp.bfloat16).reshape(peer_count, slot_c...  20.5 us
    all_to_all x1, waiting for transfers between devices, expert_entry(): lax.all_to_all(own_slice, 'ep', split_axis=0, concat_axis=0, tiled=True)  17.7 us
    all_gather x1, waiting for transfers between devices, expert_exit(): lax.all_gather(jnp.concatenate([routed_hidden, shared_hidden], axis=1), '...  15 us
    reshape x6, local copies, waits for them, and re-layouts, by_block(): return matrix.astype(jnp.float32).reshape(block_count, span, head_count,...  12.2 us
    all_gather x1, waiting for transfers between devices, mixer_part(): everything = lax.all_gather(whole.astype(jnp.bfloat16), 'ep')  9.73 us
    all_to_all x1, starting transfers between devices, expert_entry(): lax.all_to_all(own_slice, 'ep', split_axis=0, concat_axis=0, tiled=True)  6.49 us
  transfers between devices with their start and end apart: 6, of which 5 were waited for; matrix products, arithmetic and copies ran while one was open for 27% of the time, Pallas kernels for 0%

commit v1 on v0

--- a/solution.py
+++ b/solution.py
@@ -306,7 +306,7 @@
         )
     )
     flat_rows = arrived.reshape(-1, arrived.shape[2])
-    pieces = lax.all_gather(flat_rows, "tp", axis=1, tiled=True)
+    pieces = jnp.concatenate(lax.all_gather(flat_rows, "tp"), axis=1)
     token_mixer_output, pieces = mixer_part(
         receptance,
         key_tensor,

time: 223 us -> 226 us (1.013)
  local copies, waits for them, and re-layouts: 37.2 us -> 41.9 us
    all_gather x0 -> x1, local copies, waits for them, and re-layouts: none -> 4.65 us  [on_device(): pieces = jnp.concatenate(lax.all_gather(flat_rows, 'tp'), axis=1)]
where the time goes in v1:
time: 226 us; the launch traced here: 225 us
  waiting for transfers between devices  86.8 us (38%)
  matrix products  53.7 us (24%)
  local copies, waits for them, and re-layouts  41.9 us (19%)
  other arithmetic  15.9 us (7%)
  between operations  14.6 us (6%)
  starting transfers between devices  11.9 us (5%)
    dot_general x30, matrix products, product(): jnp.einsum(spec, left, right, precision=PRECISION, preferred_element_type...  32.8 us
    all_gather x1, waiting for transfers between devices, on_device(): pieces = jnp.concatenate(lax.all_gather(flat_rows, 'tp'), axis=1)  25.8 us
    all_to_all x1, waiting for transfers between devices, expert_exit(): lax.all_to_all(routed_sum.astype(jnp.bfloat16).reshape(peer_count, slot_c...  20.5 us
    all_to_all x1, waiting for transfers between devices, expert_entry(): lax.all_to_all(own_slice, 'ep', split_axis=0, concat_axis=0, tiled=True)  17.7 us
    all_gather x1, waiting for transfers between devices, expert_exit(): lax.all_gather(jnp.concatenate([routed_hidden, shared_hidden], axis=1), '...  15 us
    reshape x6, local copies, waits for them, and re-layouts, by_block(): return matrix.astype(jnp.float32).reshape(block_count, span, head_count,...  12.2 us
    all_gather x1, waiting for transfers between devices, mixer_part(): everything = lax.all_gather(whole.astype(jnp.bfloat16), 'ep')  7.68 us
    all_to_all x1, starting transfers between devices, expert_entry(): lax.all_to_all(own_slice, 'ep', split_axis=0, concat_axis=0, tiled=True)  6.49 us
  transfers between devices with their start and end apart: 6, of which 5 were waited for; matrix products, arithmetic and copies ran while one was open for 27% of the time, Pallas kernels for 0%

profile of v1, /device:TPU:0, one launch (start us, length us, event | category | flops | bytes accessed | tf_op | source)
XLA Modules:
  0.0 224.8 jit_solution(2690978383310759128)
XLA Ops:
  10.8 2.4 %scatter_custom_fusion = s32[768]{0:T(1024)S(1)} fusion(s32[512]{0:T(512)S(1)} %bitcast.196, s32[512]{0:T(512)S(1)} %add_select_fusion, s32[]{:T(128)} %constant.328.clone.1), kind=kCustom, calls=%fused_computation.207 | custom fusion | bytes 3076 | tf_op jit(solution)/shard_map/scatter | solution.py:217
  15.9 4.3 %gather_fusion = bf16[768,2048]{1,0:T(8,128)(2,1)} fusion(bf16[129,2048]{1,0:T(8,128)(2,1)S(1)} %concatenate.33, s32[1024]{0:T(1024)S(1)} %pad_clamp_fusion.1), kind=kCustom, calls=%fused_computation | custom fusion | bytes 6294528 | tf_op jit(solution)/shard_map/jit(_take)/gather | solution.py:219
  20.2 2.3 %dynamic-slice_select_fusion = bf16[8,96,512]{2,1,0:T(8,128)(2,1)} fusion(bf16[8,96,2048]{2,1,0:T(8,128)(2,1)} %bitcast.180, s32[]{:T(128)S(6)} %select_n.364, pred[8,96]{1,0:T(8,128)(4,1)S(1)} %broadcast_in_dim.94), kind=kLoop, calls=%fused_computation.114 | loop fusion | flops 393216 | bytes 1573636 | tf_op jit(solution)/shard_map/jit(_take)/select_n | solution.py:219
  22.4 6.5 %all-to-all-start = ((bf16[8,96,512]{2,1,0:T(8,128)(2,1)}), bf16[8,96,512]{2,1,0:T(8,128)(2,1)}, u32[]{:S(2)}, u32[]{:S(2)}) async-start(bf16[8,96,512]{2,1,0:T(8,128)(2,1)} %dynamic-slice_select_fusion), calls=%async_computation | async-start | bytes 1572864 | tf_op jit(solution)/shard_map/all_to_all | solution.py:225
  29.9 2.4 %convolution_bitcast_fusion.4 = f32[256,128]{0,1:T(8,128)} fusion(bf16[128,2048]{1,0:T(8,128)(2,1)S(1)} %fusion.33, bf16[256,2048]{1,0:T(8,128)(2,1)} %param.37), kind=kOutput, calls=%fused_computation.60 | convolution fusion | flops 134217728 | bytes 1703936 | tf_op jit(solution)/shard_map/fd,rd->fr/dot_general | solution.py:187
  32.3 17.7 %all-to-all-done = bf16[8,96,512]{2,1,0:T(8,128)(2,1)} async-done(((bf16[8,96,512]{2,1,0:T(8,128)(2,1)}), bf16[8,96,512]{2,1,0:T(8,128)(2,1)}, u32[]{:S(2)}, u32[]{:S(2)}) %all-to-all-start) | async-done | bytes 786464 | tf_op jit(solution)/shard_map/all_to_all | solution.py:225
  51.0 2.1 add_divide_fusion
  57.6 2.2 reshape.837
  59.8 2.4 %reshape.888 = f32[4,64,8,64]{1,0,3,2:T(4,128)} reshape(bf16[256,512]{0,1:T(8,128)(2,1)} %copy.339) | data formatting | bytes 786432 | tf_op jit(solution)/shard_map/reshape | solution.py:96
  62.2 2.6 %copy.341 = f32[4,64,8,64]{3,1,2,0:T(8,128)} copy(f32[4,64,8,64]{1,0,3,2:T(4,128)} %reshape.888) | data formatting | bytes 1048576 | tf_op jit(solution)/shard_map/reshape | solution.py:96
  64.8 5.0 %fusion.66 = (f32[4,8,64,64]{3,2,1,0:T(8,128)S(1)}, f32[4,8,64,64]{3,2,1,0:T(8,128)S(1)}, f32[4,8,64,64]{3,2,1,0:T(8,128)S(1)}, f32[4,8,64,64]{3,2,1,0:T(8,128)S(1)}, f32[4,8,64,64]{3,2,1,0:T(8,128)}) fusion(f32[4,64,8,64]{3,2,1,0:T(8,128)} %reshape.846, f32[4,8,64]{2,1,0:T(8,128)S(1)} %add_rsqrt_fusion.1, f32[4,64,8,64]{3,1,2,0:T(8,128)S(1)} %copy.345, ...), kind=kOutput, calls=%fused_computation.113 | convolution fusion | flops 101715968 | bytes 4726784 | tf_op jit(solution)/shard_map/ts,nhsd->nhtd/dot_general | solution.py:106
  69.8 2.3 %fusion.1 = f32[4,8,128,128]{3,2,1,0:T(8,128)S(1)} fusion(f32[4,8,64,64]{3,2,1,0:T(8,128)S(1)} %get-tuple-element.30, f32[4,8,64,64]{3,2,1,0:T(8,128)S(1)} %get-tuple-element.19, f32[4,8,64,64]{3,2,1,0:T(8,128)S(1)} %get-tuple-element.18, f32[4,8,64,64]{3,2,1,0:T(8,128)S(1)} %get-tuple-element.24), kind=kOutput, calls=%fused_computation.5 | convolution fusion | flops 201850880 | bytes 4194304 | tf_op jit(solution)/shard_map/nhtd,nhsd->nhts/dot_general | solution.py:47
  79.9 2.6 %fusion.8 = f32[4,8,128,64]{3,2,1,0:T(8,128)S(1)} fusion(f32[4,8,64,64]{3,2,1,0:T(8,128)} %get-tuple-element.23, f32[4,8,64,64]{3,2,1,0:T(8,128)} %get-tuple-element.22, bf16[4,8,64,64]{3,1,2,0:T(8,128)(2,1)} %bitcast.181), kind=kOutput, calls=%fused_computation.12 | convolution fusion | flops 100925440 | bytes 2359296 | tf_op jit(solution)/shard_map/nhts,nhsd->nhtd/dot_general | solution.py:47
  96.7 25.8 %all-gather.5.cloned.1.call-done = bf16[4,768,512]{2,1,0:T(8,128)(2,1)} async-done(((bf16[1,768,512]{2,1,0:T(8,128)(2,1)}), bf16[4,768,512]{2,1,0:T(8,128)(2,1)}) %all-gather.5.cloned.1.call-update) | async-done | bytes 3145744 | tf_op jit(solution)/shard_map/all_gather | solution.py:309
  122.5 4.6 %copy.360 = bf16[4,768,512]{1,2,0:T(8,128)(2,1)} copy(bf16[4,768,512]{2,1,0:T(8,128)(2,1)} %all-gather.5.cloned.1.call-done) | data formatting | bytes 6291456 | tf_op jit(solution)/shard_map/all_gather | solution.py:309
  127.5 2.5 %fusion.30 = bf16[256,128]{0,1:T(8,128)(2,1)} fusion(bf16[128,2048]{1,0:T(8,128)(2,1)} %copy-done.14, bf16[256,2048]{1,0:T(8,128)(2,1)} %param.38, f32[256,128]{0,1:T(8,128)S(1)} %copy-done.20), kind=kOutput, calls=%fused_computation.61 | convolution fusion | flops 134414336 | bytes 1769472 | tf_op jit(solution)/shard_map/fd,rd->fr/dot_general | solution.py:188
  134.8 3.9 %convolution_subtract_fusion.6 = f32[4,8,64,128]{3,2,1,0:T(8,128)} fusion(f32[4,8,64,128]{3,2,1,0:T(8,128)} %copy-done.10, f32[4,8,128,128]{3,2,1,0:T(8,128)} %copy-done.1, f32[4,8,64,64]{3,2,1,0:T(8,128)} %get-tuple-element.20, f32[4,8,64,64]{3,2,1,0:T(8,128)S(1)} %copy-done.9, pred[64,64]{1,0:T(8,128)(4,1)S(1)} %iota_compare_fusion.2), kind=kOutput, calls=%fused_computation.27 | convolution fusion | flops 101318656 | bytes 4722688 | tf_op jit(solution)/shard_map/nhts,nhsd->nhtd/dot_general | solution.py:47
  141.9 7.7 %all-gather.9.cloned.1.call-done = bf16[64,64,128]{2,1,0:T(8,128)(2,1)} async-done(((bf16[8,64,128]{2,1,0:T(8,128)(2,1)}), bf16[64,64,128]{2,1,0:T(8,128)(2,1)}) %all-gather.9.cloned.1.call-update) | async-done | bytes 1048592 | tf_op jit(solution)/shard_map/all_gather | solution.py:146
  165.6 3.2 %convolution_convert_fusion = bf16[256,2048]{1,0:T(8,128)(2,1)} fusion(bf16[512,2048]{1,0:T(8,128)(2,1)S(1)} %copy-done, bf16[256,512]{1,0:T(8,128)(2,1)} %param.25, f32[256,512]{1,0:T(8,128)} %copy.368, bf16[256,512]{1,0:T(8,128)(2,1)S(1)} %copy-done.17, f32[256,512]{1,0:T(8,128)} %copy.367, f32[256,512]{1,0:T(8,128)} %reshape.842, ...), kind=kOutput, calls=%fused_computation.4 | convolution fusion | flops 538574848 | bytes 5769216 | tf_op jit(solution)/shard_map/dot_general | solution.py:176
  168.9 15.0 %all-gather.7.cloned.1.call-done = bf16[1024,896]{0,1:T(8,128)(2,1)} async-done(((bf16[256,896]{0,1:T(8,128)(2,1)}), bf16[1024,896]{0,1:T(8,128)(2,1)}) %all-gather.7.cloned.1.call-update) | async-done | bytes 1835024 | tf_op jit(solution)/shard_map/all_gather | solution.py:248
  183.9 3.6 %fusion.14 = bf16[768,512]{1,0:T(8,128)(2,1)} fusion(bf16[1024,896]{0,1:T(8,128)(2,1)} %all-gather.7.cloned.1.call-done, bf16[1,1024,512]{2,1,0:T(8,128)(2,1)} %param.36), kind=kOutput, calls=%fused_computation.23 | convolution fusion | flops 805699584 | bytes 3407872 | tf_op jit(solution)/shard_map/fr,fd->rd/dot_general | solution.py:253
  187.4 4.6 %all-to-all-start.1 = ((bf16[8,96,512]{2,1,0:T(8,128)(2,1)}), bf16[8,96,512]{2,1,0:T(8,128)(2,1)S(1)}, u32[]{:S(2)}, u32[]{:S(2)}) async-start(bf16[8,96,512]{2,1,0:T(8,128)(2,1)} %bitcast.191), calls=%async_computation.2 | async-start | bytes 1572864 | tf_op jit(solution)/shard_map/all_to_all | solution.py:257
  192.5 20.5 %all-to-all-done.1 = bf16[8,96,512]{2,1,0:T(8,128)(2,1)S(1)} async-done(((bf16[8,96,512]{2,1,0:T(8,128)(2,1)}), bf16[8,96,512]{2,1,0:T(8,128)(2,1)S(1)}, u32[]{:S(2)}, u32[]{:S(2)}) %all-to-all-start.1) | async-done | bytes 786464 | tf_op jit(solution)/shard_map/all_to_all | solution.py:257
  216.0 2.3 %fusion.28 = bf16[128,512]{1,0:T(8,128)(2,1)} fusion(f32[128,512]{1,0:T(8,128)S(1)} %multiply_reduce_fusion, bf16[1024,512]{1,0:T(8,128)(2,1)} %param.39, bf16[1024,896]{0,1:T(8,128)(2,1)} %all-gather.7.cloned.1.call-done), kind=kOutput, calls=%fused_computation.57 | convolution fusion | flops 134348800 | bytes 1703936 | tf_op jit(solution)/shard_map/fr,fd->rd/dot_general | solution.py:254
  (176 shorter events, 61.7 us)
Async XLA Ops:
  7.2 158.4 %copy-start = (bf16[512,2048]{1,0:T(8,128)(2,1)S(1)}, bf16[512,2048]{1,0:T(8,128)(2,1)}, u32[]{:S(2)}) copy-start(bf16[512,2048]{1,0:T(8,128)(2,1)} %param.29) | copy-start | bytes 6291460
  15.8 14.1 %copy-start.14 = (bf16[128,2048]{1,0:T(8,128)(2,1)}, bf16[128,2048]{1,0:T(8,128)(2,1)S(1)}, u32[]{:S(2)}) copy-start(bf16[128,2048]{1,0:T(8,128)(2,1)S(1)} %fusion.33) | copy-start | bytes 1572868
  22.4 27.5 %copy-start.18 = (bf16[256,512]{1,0:T(8,128)(2,1)S(1)}, bf16[256,512]{1,0:T(8,128)(2,1)}, u32[]{:S(2)}) copy-start(bf16[256,512]{1,0:T(8,128)(2,1)} %param.21) | copy-start | bytes 786436
  22.4 27.7 %copy-start.19 = (bf16[256,512]{1,0:T(8,128)(2,1)S(1)}, bf16[256,512]{1,0:T(8,128)(2,1)}, u32[]{:S(2)}) copy-start(bf16[256,512]{1,0:T(8,128)(2,1)} %param.20) | copy-start | bytes 786436
  22.4 28.5 %copy-start.23 = (f32[512]{0:T(512)S(1)}, f32[512]{0:T(512)}, u32[]{:S(2)}) copy-start(f32[512]{0:T(512)} %param.26) | copy-start | bytes 6148
  22.4 27.5 %all-to-all-start = ((bf16[8,96,512]{2,1,0:T(8,128)(2,1)}), bf16[8,96,512]{2,1,0:T(8,128)(2,1)}, u32[]{:S(2)}, u32[]{:S(2)}) async-start(bf16[8,96,512]{2,1,0:T(8,128)(2,1)} %dynamic-slice_select_fusion), calls=%async_computation | async-start | bytes 1572864 | tf_op jit(solution)/shard_map/all_to_all | solution.py:225
  28.9 93.6 %all-gather.5.cloned.1.call-start = ((), (), s32[]{:S(2)}) async-start(), calls=%async_computation.3 | async-start | bytes 3932160 | tf_op jit(solution)/shard_map/all_gather | solution.py:309
  72.1 2.8 %copy-start.1 = (f32[4,8,128,128]{3,2,1,0:T(8,128)}, f32[4,8,128,128]{3,2,1,0:T(8,128)S(1)}, u32[]{:S(2)}) copy-start(f32[4,8,128,128]{3,2,1,0:T(8,128)S(1)} %fusion.1) | copy-start | bytes 6291460
  79.6 70.0 %all-gather.9.cloned.1.call-start = ((), (), s32[]{:S(2)}) async-start(), calls=%async_computation.6 | async-start | bytes 1179648 | tf_op jit(solution)/shard_map/all_gather | solution.py:146
  79.8 2.8 %copy-start.2 = (f32[4,8,128,128]{3,2,1,0:T(8,128)S(1)}, f32[4,8,128,128]{3,2,1,0:T(8,128)}, u32[]{:S(2)}) copy-start(f32[4,8,128,128]{3,2,1,0:T(8,128)} %copy-done.1) | copy-start | bytes 6291460
  91.2 3.5 %copy-start.10 = (f32[4,8,64,128]{3,2,1,0:T(8,128)}, f32[4,8,64,128]{3,2,1,0:T(8,128)S(1)}, u32[]{:S(2)}) copy-start(f32[4,8,64,128]{3,2,1,0:T(8,128)S(1)} %fusion.35) | copy-start | bytes 3145732
  96.7 30.8 %copy-start.20 = (f32[256,128]{0,1:T(8,128)S(1)}, f32[256,128]{0,1:T(8,128)}, u32[]{:S(2)}) copy-start(f32[256,128]{0,1:T(8,128)} %convolution_bitcast_fusion.4) | copy-start | bytes 393220
  127.2 7.6 %copy-start.9 = (f32[4,8,64,64]{3,2,1,0:T(8,128)S(1)}, f32[4,8,64,64]{3,2,1,0:T(8,128)}, u32[]{:S(2)}) copy-start(f32[4,8,64,64]{3,2,1,0:T(8,128)} %copy-done.8) | copy-start | bytes 1572868
  127.2 56.7 %all-gather.7.cloned.1.call-start = ((), (), s32[]{:S(2)}) async-start(), calls=%async_computation.5 | async-start | bytes 2293760 | tf_op jit(solution)/shard_map/all_gather | solution.py:248
  134.8 3.9 %copy-start.16 = (bf16[4,768,512]{1,2,0:T(8,128)(2,1)S(1)}, bf16[4,768,512]{1,2,0:T(8,128)(2,1)}, u32[]{:S(2)}) copy-start(bf16[4,768,512]{1,2,0:T(8,128)(2,1)} %copy.360) | copy-start | bytes 9437188
  134.8 3.9 %copy-start.26 = (bf16[1,256,2048]{2,1,0:T(8,128)(2,1)S(1)}, bf16[1,256,2048]{2,1,0:T(8,128)(2,1)}, u32[]{:S(2)}) copy-start(bf16[1,256,2048]{2,1,0:T(8,128)(2,1)} %param.34) | copy-start | bytes 3145732
  141.8 16.3 %copy-start.4 = (f32[4,8,64,128]{3,2,1,0:T(8,128)S(1)}, f32[4,8,64,128]{3,2,1,0:T(8,128)}, u32[]{:S(2)}) copy-start(f32[4,8,64,128]{3,2,1,0:T(8,128)} %copy-done.3) | copy-start | bytes 3145732
  141.8 76.4 %reduce-scatter.2.cloned.1.call-start = ((), (), s32[]{:S(2)}) async-start(), calls=%async_computation.4 | async-start | bytes 1310720 | tf_op jit(solution)/shard_map/reduce_scatter | solution.py:175
  154.4 4.5 %copy-start.15 = (f32[4,8,64,128]{3,2,1,0:T(8,128)S(1)}, f32[4,8,64,128]{3,2,1,0:T(8,128)}, u32[]{:S(2)}) copy-start(f32[4,8,64,128]{3,2,1,0:T(8,128)} %convolution_subtract_fusion.6) | copy-start | bytes 3145732
  162.1 3.5 %copy-start.17 = (bf16[256,512]{1,0:T(8,128)(2,1)S(1)}, bf16[256,512]{1,0:T(8,128)(2,1)}, u32[]{:S(2)}) copy-start(bf16[256,512]{1,0:T(8,128)(2,1)} %param.22) | copy-start | bytes 786436
  162.1 3.5 %copy-start.24 = (f32[512]{0:T(512)S(1)}, f32[512]{0:T(512)}, u32[]{:S(2)}) copy-start(f32[512]{0:T(512)} %param.27) | copy-start | bytes 6148
  168.8 23.3 %copy-start.25 = (f32[128,4]{0,1:T(4,128)S(1)}, f32[128,4]{0,1:T(4,128)}, u32[]{:S(2)}) copy-start(f32[128,4]{0,1:T(4,128)} %param.32) | copy-start | bytes 6148
  168.9 23.5 %copy-start.22 = (s32[128,4]{0,1:T(4,128)S(1)}, s32[128,4]{0,1:T(4,128)}, u32[]{:S(2)}) copy-start(s32[128,4]{0,1:T(4,128)} %param.31) | copy-start | bytes 6148
  187.4 25.5 %all-to-all-start.1 = ((bf16[8,96,512]{2,1,0:T(8,128)(2,1)}), bf16[8,96,512]{2,1,0:T(8,128)(2,1)S(1)}, u32[]{:S(2)}, u32[]{:S(2)}) async-start(bf16[8,96,512]{2,1,0:T(8,128)(2,1)} %bitcast.191), calls=%async_computation.2 | async-start | bytes 1572864 | tf_op jit(solution)/shard_map/all_to_all | solution.py:257
  (10 other events, 16.6 us)
Sparse Core Ops, SparseCore 0:
  79.7 42.7 all-gather.4
  127.3 22.2 all-gather.8
  151.4 32.4 all-gather.6
  187.2 27.9 reduce-scatter.1
